TPU v7x, 256 devices: a 4x2x16 block of a 4x16x16 slice. The times are simulated.
256 devices in a mesh: grp: 2 (over y), fs: 16 (over z), tp: 8 (over x, core).
Axes of the slice: x: 4, y: 2, z: 16, core: 2. Of those that a mesh axis runs over, the one named last changes fastest.
The devices are a block of a 4x16x16 slice.
Arguments:
- tokens: bfloat16 [8192, 2048], P(('grp', 'fs')), parts along dimension 0, may hold values from -6 to 6
- route_ids: int32 [8192, 2], P(('grp', 'fs')), parts along dimension 0, may hold values from 0 to 31, as said below
- route_weights: float32 [8192, 2], P(('grp', 'fs')), parts along dimension 0, may hold values from 0.2 to 1
- ffn_gain: float32 [2048], P('fs'), may hold values from 0.1 to 1.9
- gate_master: float32 [32, 2048, 1024], P(None, 'fs', 'tp'), may hold values from -0.125 to 0.125
- up_master: float32 [32, 2048, 1024], P(None, 'fs', 'tp'), may hold values from -0.125 to 0.125
- down_master: float32 [32, 1024, 2048], P(None, 'fs', 'tp'), may hold values from -0.1875 to 0.1875
Outputs:
- gate_serve: bfloat16 [64, 2048, 1024], P(('grp', 'fs'), None, 'tp'), parts along dimension 0
- up_serve: bfloat16 [64, 2048, 1024], P(('grp', 'fs'), None, 'tp'), parts along dimension 0
- down_serve: bfloat16 [64, 1024, 2048], P(('grp', 'fs'), None, 'tp'), parts along dimension 0
- mixed: bfloat16 [8192, 2048], P(('grp', 'fs'), 'tp'), parts along dimension 0
There are 2 independent parts, one for each index of `grp`. A program takes and returns all parts, laid end to end along the dimension named above; an argument that names none is the same for every part. Nothing has to cross between parts.
Inputs may be any that keep to these rules, and one draw needn't show every extreme that they name: `route_ids`: each row names two different experts of one group of 8 consecutive experts. Among the tokens of one index of fs, each group is named by exactly 64 tokens and no expert by more than 32; in every group one expert, the same for every index of fs, is named by exactly 32, and so is one other expert of the group, which may change from one index of fs to the next.
All inputs are finite; a program needn't handle non-finite values.
Results may differ from a plain program's by a relative error of at most 0.0087.
Values may be sent and summed in bfloat16 or wider, within the bound.
A program may use at most 64 MiB of HBM per device.

v0:
```python
import jax
import jax.numpy as jnp
from jax import lax
from jax.sharding import Mesh
from jax.sharding import PartitionSpec as P

GROUP_SIZE = 8
TP = ("tp_0", "tp_1")


def in_one_piece(arrays, axis, split_dim, concat_dim, along):
    ends, at = ([], 0)
    for a in arrays[:-1]:
        at += a.shape[along]
        ends.append(at)
    both = jnp.concatenate(arrays, axis=along)
    return tuple(
        jnp.split(
            lax.all_to_all(both, axis, split_axis=split_dim, concat_axis=concat_dim, tiled=True),
            ends,
            axis=along,
        )
    )


def laid_out(blocks, dim):
    dims = list(blocks.shape[1:])
    dims[dim] *= blocks.shape[0]
    return jnp.moveaxis(blocks, 0, dim).reshape(dims)


def gather_in_order(x, axes, turns):
    blocks = x[None]
    for k in turns:
        blocks = lax.all_gather(blocks, axes[k], axis=0, tiled=True)
    carried = [lax.axis_size(axes[k]) for k in reversed(turns)]
    blocks = blocks.reshape(*carried, *x.shape)
    turned = sorted(range(len(turns)), key=lambda place: turns[len(turns) - 1 - place])
    return blocks.transpose(*turned, *range(len(turns), blocks.ndim)).reshape(-1, *x.shape)


def gathered_by_axis(x, axes, turns, dim):
    return laid_out(gather_in_order(x, axes, turns), dim)


def slot_targets(route_ids, experts, capacity):
    flat_ids = route_ids.reshape(-1)
    member = (flat_ids[:, None] == jnp.arange(experts, dtype=jnp.int32)[None, :]).astype(jnp.int32)
    before = jnp.cumsum(member, axis=0) - member
    slot_index = jnp.sum(before * member, axis=1)
    return flat_ids * capacity + slot_index


def fill_slots(source, targets, experts, capacity):
    doubled = jnp.repeat(source, 2, axis=0)
    buffer = jnp.zeros((experts * capacity, source.shape[1]), source.dtype).at[targets].set(doubled)
    return buffer.reshape(experts, capacity, source.shape[1])


def on_device(tokens, route_ids, route_weights, ffn_gain, gate_master, up_master, down_master):
    row_gain = ffn_gain[None, :, None]
    gate_local = (gate_master * row_gain).astype(jnp.bfloat16)
    up_local = (up_master * row_gain).astype(jnp.bfloat16)
    down_local = down_master.astype(jnp.bfloat16)
    gate_serve, up_serve, down_serve = (
        *in_one_piece((gate_local, up_local), "fs", 0, 1, 2),
        lax.all_to_all(down_local, "fs", split_axis=0, concat_axis=1, tiled=True),
    )
    experts = gate_local.shape[0]
    capacity = tokens.shape[0] // (2 * (experts // GROUP_SIZE))
    token_rows = tokens.astype(jnp.float32)
    normed = (
        token_rows * lax.rsqrt(jnp.mean(token_rows * token_rows, axis=1, keepdims=True) + 1e-06)
    ).astype(jnp.bfloat16)
    targets = slot_targets(route_ids, experts, capacity)
    col_width = normed.shape[1] // lax.axis_size(TP)
    own_cols = lax.dynamic_slice_in_dim(normed, lax.axis_index(TP) * col_width, col_width, 1)
    part_rows = lax.all_to_all(
        fill_slots(own_cols, targets, experts, capacity),
        "fs",
        split_axis=0,
        concat_axis=1,
        tiled=True,
    )
    portion = gathered_by_axis(part_rows, TP, (0, 1), 2)
    gate_part = jnp.einsum("erd,edf->erf", portion, gate_serve, preferred_element_type=jnp.float32)
    up_part = jnp.einsum("erd,edf->erf", portion, up_serve, preferred_element_type=jnp.float32)
    hidden = (jax.nn.silu(gate_part) * up_part).astype(jnp.bfloat16)
    expert_out = jnp.einsum(
        "erf,efd->erd",
        gathered_by_axis(hidden, TP, (0, 1), 2),
        down_serve,
        preferred_element_type=jnp.float32,
    ).astype(jnp.bfloat16)
    returned_rows = lax.all_to_all(expert_out, "fs", split_axis=1, concat_axis=0, tiled=True)
    picked = returned_rows.reshape(-1, returned_rows.shape[2])[targets].astype(jnp.float32)
    weighted = picked * route_weights.reshape(-1, 1)
    combined = jnp.sum(weighted.reshape(-1, 2, returned_rows.shape[2]), axis=1).astype(jnp.bfloat16)
    return (gate_serve, up_serve, down_serve, combined)


def solution(mesh):
    split = Mesh(
        mesh.devices.reshape(mesh.shape["grp"], mesh.shape["fs"], 4, 2),
        ("grp", "fs", "tp_0", "tp_1"),
    )
    in_specs = (
        P(("grp", "fs"), None),
        P(("grp", "fs"), None),
        P(("grp", "fs"), None),
        P("fs"),
        P(None, "fs", TP),
        P(None, "fs", TP),
        P(None, "fs", TP),
    )
    out_specs = (
        P(("grp", "fs"), None, TP),
        P(("grp", "fs"), None, TP),
        P(("grp", "fs"), None, TP),
        P(("grp", "fs"), TP),
    )
    return jax.shard_map(
        on_device, mesh=split, in_specs=in_specs, out_specs=out_specs, check_vma=False
    )
```

profile of v0, /device:TPU:34, one launch (start us, length us, event | category | flops | bytes accessed | tf_op | source)
XLA Modules:
  0.0 300.8 jit_solution(5720126012257750511)
XLA Ops:
  7.2 1.5 convert_element_type.43
  8.8 0.3 multiply_reduce_fusion
  9.9 1.2 reduce-window.6
  11.8 3.1 %scatter_custom_fusion = bf16[1024,256]{1,0:T(8,128)(2,1)} fusion(s32[512]{0:T(512)S(1)} %bitcast.77, bf16[512,256]{1,0:T(8,128)(2,1)S(1)} %reshape.126, bf16[]{:T(256)} %constant.13.clone.1), kind=kCustom, calls=%fused_computation.12 | custom fusion | bytes 524290 | tf_op jit(solution)/shard_map/scatter | solution.py:56
  14.9 24.0 %all-to-all-start.2 = ((bf16[32,32,256]{2,1,0:T(8,128)(2,1)}), bf16[32,32,256]{2,1,0:T(8,128)(2,1)S(1)}, u32[]{:S(2)}, u32[]{:S(2)}) async-start(bf16[32,32,256]{2,1,0:T(8,128)(2,1)} %bitcast.10), calls=%async_computation.2 | async-start | bytes 1048576 | tf_op jit(solution)/shard_map/all_to_all | solution.py:78
  38.9 2.2 multiply_convert_fusion.1
  41.1 1.6 pad_maximum_fusion
  42.7 25.1 %all-to-all-done.2 = bf16[32,32,256]{2,1,0:T(8,128)(2,1)S(1)} async-done(((bf16[32,32,256]{2,1,0:T(8,128)(2,1)}), bf16[32,32,256]{2,1,0:T(8,128)(2,1)S(1)}, u32[]{:S(2)}, u32[]{:S(2)}) %all-to-all-start.2) | async-done | bytes 524320 | tf_op jit(solution)/shard_map/all_to_all | solution.py:78
  67.8 0.8 copy-done.3
  68.6 6.6 %all-to-all-start = ((bf16[32,128,256]{2,1,0:T(8,128)(2,1)}), bf16[32,128,256]{2,1,0:T(8,128)(2,1)S(1)}, u32[]{:S(2)}, u32[]{:S(2)}) async-start(bf16[32,128,256]{2,1,0:T(8,128)(2,1)} %pad_maximum_fusion), calls=%async_computation | async-start | bytes 4194304 | tf_op jit(solution)/shard_map/all_to_all | solution.py:19
  75.2 1.9 copy.43
  77.2 38.8 %all-gather.6.cloned.1.call-done = bf16[4,2,512,256]{3,2,1,0:T(8,128)(2,1)} async-done(((bf16[1,2,512,256]{3,2,1,0:T(8,128)(2,1)}), bf16[4,2,512,256]{3,2,1,0:T(8,128)(2,1)}) %all-gather.6.cloned.1.call-update) | async-done | bytes 2097168 | tf_op jit(solution)/shard_map/all_gather | solution.py:35
  116.1 2.7 convert_element_type.40
  118.8 51.4 %all-to-all-done = bf16[32,128,256]{2,1,0:T(8,128)(2,1)S(1)} async-done(((bf16[32,128,256]{2,1,0:T(8,128)(2,1)}), bf16[32,128,256]{2,1,0:T(8,128)(2,1)S(1)}, u32[]{:S(2)}, u32[]{:S(2)}) %all-to-all-start) | async-done | bytes 2097184 | tf_op jit(solution)/shard_map/all_to_all | solution.py:19
  170.2 7.9 %all-to-all-start.1 = ((bf16[32,64,256]{2,1,0:T(8,128)(2,1)}), bf16[32,64,256]{2,1,0:T(8,128)(2,1)S(1)}, u32[]{:S(2)}, u32[]{:S(2)}) async-start(bf16[32,64,256]{2,1,0:T(8,128)(2,1)} %convert_element_type.40), calls=%async_computation.1 | async-start | bytes 2097152 | tf_op jit(solution)/shard_map/all_to_all | solution.py:67
  178.3 0.4 fusion.8
  178.7 3.2 %copy.44 = bf16[4,2,2,512,256]{4,3,2,1,0:T(8,128)(2,1)S(1)} copy(bf16[4,2,2,512,256]{4,3,2,0,1:T(8,128)(2,1)} %bitcast.68) | data formatting | bytes 8388608 | tf_op jit(solution)/shard_map/transpose | solution.py:39
  181.9 0.6 copy.51
  182.5 1.3 fusion.9
  183.8 2.0 fusion
  186.1 30.3 %all-gather.12.cloned.1.call-done = bf16[8,512,128]{2,1,0:T(8,128)(2,1)} async-done(((bf16[2,512,128]{2,1,0:T(8,128)(2,1)}), bf16[8,512,128]{2,1,0:T(8,128)(2,1)}) %all-gather.12.cloned.1.call-update) | async-done | bytes 1048592 | tf_op jit(solution)/shard_map/all_gather | solution.py:35
  216.4 11.6 %all-to-all-done.1 = bf16[32,64,256]{2,1,0:T(8,128)(2,1)S(1)} async-done(((bf16[32,64,256]{2,1,0:T(8,128)(2,1)}), bf16[32,64,256]{2,1,0:T(8,128)(2,1)S(1)}, u32[]{:S(2)}, u32[]{:S(2)}) %all-to-all-start.1) | async-done | bytes 1048608 | tf_op jit(solution)/shard_map/all_to_all | solution.py:67
  228.1 11.3 %all-gather.10.cloned.1.call-done = bf16[8,2,512,128]{3,2,1,0:T(8,128)(2,1)} async-done(((bf16[4,2,512,128]{3,2,1,0:T(8,128)(2,1)}), bf16[8,2,512,128]{3,2,1,0:T(8,128)(2,1)}) %all-gather.10.cloned.1.call-update) | async-done | bytes 2097168 | tf_op jit(solution)/shard_map/all_gather | solution.py:35
  239.4 3.7 %copy.46 = bf16[4,2,2,512,128]{4,1,0,3,2:T(2,128)(2,1)S(1)} copy(bf16[4,2,2,512,128]{4,3,2,0,1:T(8,128)(2,1)} %bitcast.70) | data formatting | bytes 4194304 | tf_op jit(solution)/shard_map/transpose | solution.py:39
  243.2 2.3 reshape.111
  245.5 2.3 convolution_convert_fusion
  247.8 1.3 copy.47
  249.1 12.4 %all-to-all-start.3 = ((bf16[2,512,256]{2,0,1:T(2,128)(2,1)}), bf16[2,512,256]{2,0,1:T(2,128)(2,1)S(1)}, u32[]{:S(2)}, u32[]{:S(2)}) async-start(bf16[2,512,256]{2,0,1:T(2,128)(2,1)} %copy.47), calls=%async_computation.3 | async-start | bytes 1048576 | tf_op jit(solution)/shard_map/all_to_all | solution.py:95
  261.6 28.9 %all-to-all-done.3 = bf16[2,512,256]{2,0,1:T(2,128)(2,1)S(1)} async-done(((bf16[2,512,256]{2,0,1:T(2,128)(2,1)}), bf16[2,512,256]{2,0,1:T(2,128)(2,1)S(1)}, u32[]{:S(2)}, u32[]{:S(2)}) %all-to-all-start.3) | async-done | bytes 524320 | tf_op jit(solution)/shard_map/all_to_all | solution.py:95
  290.7 2.0 gather_fusion
  292.6 0.3 reshape.113
  292.9 1.4 multiply_reduce_fusion.1
  (47 shorter events, 2.6 us)
Async XLA Ops:
  7.2 1.6 copy-start
  7.2 1.9 copy-start.6
  9.1 29.8 %copy-start.8 = (f32[128]{0:T(128)S(1)}, f32[128]{0:T(128)}, u32[]{:S(2)}) copy-start(f32[128]{0:T(128)} %param.10) | copy-start | bytes 1540
  9.6 29.3 %copy-start.2 = (f32[32,128,128]{2,1,0:T(8,128)S(1)}, f32[32,128,128]{2,1,0:T(8,128)}, u32[]{:S(2)}) copy-start(f32[32,128,128]{2,1,0:T(8,128)} %param.11) | copy-start | bytes 6291460
  14.9 52.9 %all-to-all-start.2 = ((bf16[32,32,256]{2,1,0:T(8,128)(2,1)}), bf16[32,32,256]{2,1,0:T(8,128)(2,1)S(1)}, u32[]{:S(2)}, u32[]{:S(2)}) async-start(bf16[32,32,256]{2,1,0:T(8,128)(2,1)} %bitcast.10), calls=%async_computation.2 | async-start | bytes 1048576 | tf_op jit(solution)/shard_map/all_to_all | solution.py:78
  67.8 0.8 copy-start.3
  68.6 101.6 %all-to-all-start = ((bf16[32,128,256]{2,1,0:T(8,128)(2,1)}), bf16[32,128,256]{2,1,0:T(8,128)(2,1)S(1)}, u32[]{:S(2)}, u32[]{:S(2)}) async-start(bf16[32,128,256]{2,1,0:T(8,128)(2,1)} %pad_maximum_fusion), calls=%async_computation | async-start | bytes 4194304 | tf_op jit(solution)/shard_map/all_to_all | solution.py:19
  75.2 40.9 %all-gather.6.cloned.1.call-start = ((), (), s32[]{:S(2)}) async-start(), calls=%async_computation.4 | async-start | bytes 2621440 | tf_op jit(solution)/shard_map/all_gather | solution.py:35
  77.2 101.6 %all-gather.8.cloned.1.call-start = ((), (), s32[]{:S(2)}) async-start(), calls=%async_computation.5 | async-start | bytes 6291456 | tf_op jit(solution)/shard_map/all_gather | solution.py:35
  170.2 57.8 %all-to-all-start.1 = ((bf16[32,64,256]{2,1,0:T(8,128)(2,1)}), bf16[32,64,256]{2,1,0:T(8,128)(2,1)S(1)}, u32[]{:S(2)}, u32[]{:S(2)}) async-start(bf16[32,64,256]{2,1,0:T(8,128)(2,1)} %convert_element_type.40), calls=%async_computation.1 | async-start | bytes 2097152 | tf_op jit(solution)/shard_map/all_to_all | solution.py:67
  178.1 38.3 %all-gather.12.cloned.1.call-start = ((), (), s32[]{:S(2)}) async-start(), calls=%async_computation.7 | async-start | bytes 1310720 | tf_op jit(solution)/shard_map/all_gather | solution.py:35
  178.7 3.8 %copy-start.1 = (bf16[2,2048,128]{2,1,0:T(8,128)(2,1)}, bf16[2,2048,128]{2,1,0:T(8,128)(2,1)S(1)}, u32[]{:S(2)}) copy-start(bf16[2,2048,128]{2,1,0:T(8,128)(2,1)S(1)} %get-tuple-element.5) | copy-start | bytes 3145732
  178.7 5.1 %copy-start.5 = (bf16[2,2048,128]{2,1,0:T(8,128)(2,1)}, bf16[2,2048,128]{2,1,0:T(8,128)(2,1)S(1)}, u32[]{:S(2)}) copy-start(bf16[2,2048,128]{2,1,0:T(8,128)(2,1)S(1)} %get-tuple-element.4) | copy-start | bytes 3145732
  185.8 53.6 %all-gather.10.cloned.1.call-start = ((), (), s32[]{:S(2)}) async-start(), calls=%async_computation.6 | async-start | bytes 3145728 | tf_op jit(solution)/shard_map/all_gather | solution.py:35
  228.1 17.3 %copy-start.4 = (bf16[16,2,64,256]{3,2,0,1:T(8,128)(2,1)}, bf16[16,2,64,256]{3,2,0,1:T(8,128)(2,1)S(1)}, u32[]{:S(2)}) copy-start(bf16[16,2,64,256]{3,2,0,1:T(8,128)(2,1)S(1)} %copy.38) | copy-start | bytes 3145732
  245.5 16.0 %copy-start.7 = (f32[256,2]{0,1:T(2,128)S(1)}, f32[256,2]{0,1:T(2,128)}, u32[]{:S(2)}) copy-start(f32[256,2]{0,1:T(2,128)} %param.9) | copy-start | bytes 6148
  249.1 41.5 %all-to-all-start.3 = ((bf16[2,512,256]{2,0,1:T(2,128)(2,1)}), bf16[2,512,256]{2,0,1:T(2,128)(2,1)S(1)}, u32[]{:S(2)}, u32[]{:S(2)}) async-start(bf16[2,512,256]{2,0,1:T(2,128)(2,1)} %copy.47), calls=%async_computation.3 | async-start | bytes 1048576 | tf_op jit(solution)/shard_map/all_to_all | solution.py:95
Sparse Core Ops, SparseCore 0:
  78.4 37.6 all-gather.5
  117.9 23.5 all-gather.7
  185.9 30.3 all-gather.11
  218.1 21.3 all-gather.9
where the time goes:
time: 302 us; the launch traced here: 301 us
  waiting for transfers between devices  198 us (66%)
  starting transfers between devices  51.2 us (17%)
  local copies, waits for them, and re-layouts  21.2 us (7%)
  between operations  14.1 us (5%)
  other arithmetic  11.2 us (4%)
  matrix products  5.54 us (2%)
    all_gather x4, waiting for transfers between devices, gather_in_order(): blocks = lax.all_gather(blocks, axes[k], axis=0, tiled=True)  80.4 us
    all_to_all x1, waiting for transfers between devices, in_one_piece(): lax.all_to_all(both, axis, split_axis=split_dim, concat_axis=concat_dim,...  51.4 us
    all_to_all x1, waiting for transfers between devices, on_device(): lax.all_to_all(expert_out, 'fs', split_axis=1, concat_axis=0, tiled=True)  28.9 us
    all_to_all x1, waiting for transfers between devices, on_device(): lax.all_to_all(fill_slots(own_cols, targets, experts, capacity), 'fs', sp...  25.1 us
    all_to_all x1, starting transfers between devices, on_device(): lax.all_to_all(fill_slots(own_cols, targets, experts, capacity), 'fs', sp...  24 us
    all_to_all x1, starting transfers between devices, on_device(): lax.all_to_all(expert_out, 'fs', split_axis=1, concat_axis=0, tiled=True)  12.4 us
    all_to_all x1, waiting for transfers between devices, on_device(): lax.all_to_all(down_local, 'fs', split_axis=0, concat_axis=1, tiled=True)  11.6 us
    all_to_all x1, starting transfers between devices, on_device(): lax.all_to_all(down_local, 'fs', split_axis=0, concat_axis=1, tiled=True)  7.88 us
  transfers between devices with their start and end apart: 8, of which 7 were waited for; matrix products, arithmetic and copies ran while one was open for 5% of the time, Pallas kernels for 0%

commit v1 on v0

v1 whole, which is shorter than its diff:
```python
import functools

import jax
import jax.numpy as jnp
from jax import lax
from jax.experimental import pallas as pl
from jax.experimental.pallas import tpu as pltpu
from jax.sharding import PartitionSpec as P

GROUP_SIZE = 8
MESH = pl.DeviceIdType.MESH
BF16 = jnp.bfloat16
F32 = jnp.float32


def remote(src, dst, send, recv, where):
    return pltpu.make_async_remote_copy(
        src_ref=src, dst_ref=dst, send_sem=send, recv_sem=recv, device_id=where, device_id_type=MESH
    )


def kernel(
    n_fs, n_tp, span,
    tok_ref, ids_ref, rw_ref, gain_ref, gm_ref, um_ref, dm_ref,
    og_out, ou_out, od_out, mix_ref,
    g_in, u_in, d_in, g_own, u_own, d_own,
    g_send, u_send, d_send, og, ou, od,
    s_buf, w_send, x_buf, w_recv, h_buf, w_rows, part, gathered, total, final,
    load_sem, out_sem, z_send, z_recv, y_send, y_recv, tz_send, tz_recv,
    xs_sem, xr_sem, hs_sem, hr_sem, ps_sem, pr_sem, fs_sem, fr_sem,
):
    grp, me, t = lax.axis_index("grp"), lax.axis_index("fs"), lax.axis_index("tp")
    q = lax.rem(grp, 2)
    other = 1 - q
    mate = grp + 1 - 2 * q
    right, left = lax.rem(t + 2, n_tp), lax.rem(t + n_tp - 2, n_tp)
    far = lax.rem(t + 4, n_tp)
    twin = t + 1 - 2 * lax.rem(t, 2)
    member = lax.rem(me, span)
    base = me - member
    toks = tok_ref.shape[0]
    cols = s_buf.shape[1]
    per = s_buf.shape[0] // (n_fs // span)
    quarter = per // span

    def turn(i):
        half = lax.div(i, 2)
        odd = lax.rem(i, 2)
        return half + 1 + odd * (n_fs - 2 * half - 2)

    barrier = pltpu.get_barrier_semaphore()

    def greet(i, c):
        pl.semaphore_signal(
            barrier, inc=1, device_id={"fs": lax.rem(me + i, n_fs)}, device_id_type=MESH
        )
        return c

    lax.fori_loop(1, n_fs, greet, 0)
    pl.semaphore_signal(barrier, inc=1, device_id={"grp": mate}, device_id_type=MESH)
    for peer in (right, left, twin):
        pl.semaphore_signal(barrier, inc=1, device_id={"tp": peer}, device_id_type=MESH)

    loads = [
        pltpu.make_async_copy(gm_ref.at[:, q], g_in, load_sem.at[0]),
        pltpu.make_async_copy(um_ref.at[:, q], u_in, load_sem.at[1]),
        pltpu.make_async_copy(dm_ref.at[:, q], d_in, load_sem.at[2]),
        pltpu.make_async_copy(gm_ref.at[me, other], g_own, load_sem.at[3]),
        pltpu.make_async_copy(um_ref.at[me, other], u_own, load_sem.at[4]),
        pltpu.make_async_copy(dm_ref.at[me, other], d_own, load_sem.at[5]),
    ]
    for load in loads:
        load.start()

    ids = ids_ref[...]
    group = lax.shift_right_logical(ids[:, 0:1], GROUP_SIZE.bit_length() - 1)
    lane = lax.broadcasted_iota(jnp.int32, (toks, 128), 1)
    group_hot = (group == lane).astype(F32)
    row = lax.broadcasted_iota(jnp.int32, (toks, toks), 0)
    col = lax.broadcasted_iota(jnp.int32, (toks, toks), 1)
    earlier = (col < row).astype(BF16)
    counts = jnp.dot(earlier, group_hot.astype(BF16), preferred_element_type=F32)
    rank = jnp.sum(counts * group_hot, axis=1, keepdims=True)
    target = group.astype(F32) * per + rank
    place = (target == col.astype(F32)).astype(BF16)
    tok = tok_ref[...].astype(F32)
    scale = lax.rsqrt(jnp.mean(tok * tok, axis=1, keepdims=True) + 1e-06)
    own = tok_ref[:, pl.ds(pl.multiple_of(t * cols, cols), cols)].astype(F32)
    normed = (own * scale).astype(BF16)
    s_buf[...] = lax.dot_general(
        place, normed, (((0,), (0,)), ((), ())), preferred_element_type=F32
    ).astype(BF16)
    rw = rw_ref[...]
    by_expert = jnp.where(ids[:, 0:1] == lane, rw[:, 0:1], 0.0) + jnp.where(
        ids[:, 1:2] == lane, rw[:, 1:2], 0.0
    )
    rank_hot = (rank == lane.astype(F32)).astype(F32)
    w_all = lax.dot_general(
        by_expert, rank_hot, (((0,), (0,)), ((), ())),
        preferred_element_type=F32, precision=lax.Precision.HIGHEST,
    )
    for j in range(n_fs):
        w_send[j] = w_all[2 * j : 2 * j + 2]

    pl.semaphore_wait(barrier, n_fs - 1 + 4)

    def rows_at(buf, s):
        half = x_buf.shape[2] // per
        return buf.at[t, lax.div(s, half), pl.ds(pl.multiple_of(lax.rem(s, half) * per, per), per)]

    def tok_copy(j, s):
        begin = pl.multiple_of(lax.div(j, span) * per, per)
        return remote(
            s_buf.at[pl.ds(begin, per)], rows_at(x_buf, s), tz_send.at[0, j], tz_recv.at[0, s], {"fs": j}
        )

    def w_copy(j, s):
        return remote(w_send.at[j], w_recv.at[s], tz_send.at[1, j], tz_recv.at[1, s], {"fs": j})

    def dispatch(i, c):
        j = lax.rem(me + turn(i), n_fs)
        tok_copy(j, me).start()
        w_copy(j, me).start()
        return c

    lax.fori_loop(0, n_fs - 1, dispatch, 0)

    gain = jnp.broadcast_to(gain_ref[...], g_own.shape)
    gate_rows, down_rows = g_own.shape[0], d_own.shape[0]

    def gate_at(buf, e, s):
        return buf.at[e, pl.ds(pl.multiple_of(s * gate_rows, gate_rows), gate_rows)]

    def down_at(buf, e, s):
        return buf.at[e, pl.ds(pl.multiple_of(s * down_rows, down_rows), down_rows)]

    def z_copy(a, j, s):
        src = (g_send, u_send, d_send)[a].at[j]
        dst = (gate_at(og, q, s), gate_at(ou, q, s), down_at(od, q, s))[a]
        return remote(src, dst, z_send.at[a, j], z_recv.at[a, s], {"fs": j})

    def y_copy(a, e, s):
        spot = (gate_at(og, e, s), gate_at(ou, e, s), down_at(od, e, s))[a]
        return remote(spot, spot, y_send.at[a, s], y_recv.at[a, s], {"grp": mate})

    loads[0].wait()
    loads[1].wait()

    def send_gate_up(i, c):
        j = lax.rem(me + turn(i), n_fs)
        g_send[j] = (g_in[j] * gain).astype(BF16)
        u_send[j] = (u_in[j] * gain).astype(BF16)
        z_copy(0, j, me).start()
        z_copy(1, j, me).start()
        return c

    lax.fori_loop(0, n_fs - 1, send_gate_up, 0)
    for load in loads[2:]:
        load.wait()
    gate_spot = pl.ds(pl.multiple_of(me * gate_rows, gate_rows), gate_rows)
    down_spot = pl.ds(pl.multiple_of(me * down_rows, down_rows), down_rows)
    og[q, gate_spot] = (g_in[me] * gain).astype(BF16)
    ou[q, gate_spot] = (u_in[me] * gain).astype(BF16)
    od[q, down_spot] = d_in[me].astype(BF16)
    og[other, gate_spot] = (g_own[...] * gain).astype(BF16)
    ou[other, gate_spot] = (u_own[...] * gain).astype(BF16)
    od[other, down_spot] = d_own[...].astype(BF16)

    def send_down(i, c):
        j = lax.rem(me + turn(i), n_fs)
        d_send[j] = d_in[j].astype(BF16)
        z_copy(2, j, me).start()
        return c

    lax.fori_loop(0, n_fs - 1, send_down, 0)

    own_rows = s_buf[pl.ds(pl.multiple_of(lax.div(me, span) * per, per), per)]
    x_half = x_buf.shape[2] // per
    x_buf[t, lax.div(me, x_half), pl.ds(pl.multiple_of(lax.rem(me, x_half) * per, per), per)] = own_rows
    w_recv[me] = w_send[me]

    def tokens_in(i, c):
        s = lax.rem(me + n_fs - turn(i), n_fs)
        tok_copy(s, s).wait_recv()
        w_copy(s, s).wait_recv()
        return c

    lax.fori_loop(0, n_fs - 1, tokens_in, 0)

    def tp_gather(buf, send, recv):
        def to(block, k, peer):
            return remote(block, block, send.at[k], recv.at[k], {"tp": peer})

        first = [to(buf.at[t], 0, right), to(buf.at[t], 1, left), to(buf.at[t], 4, twin)]
        for copy in first:
            copy.start()
        to(buf.at[left], 0, right).wait_recv()
        second = [to(buf.at[left, 0], 2, right), to(buf.at[left], 5, twin)]
        for copy in second:
            copy.start()
        to(buf.at[right], 1, left).wait_recv()
        third = [to(buf.at[right, 1], 3, left), to(buf.at[right], 6, twin)]
        for copy in third:
            copy.start()
        to(buf.at[far, 0], 2, right).wait_recv()
        to(buf.at[far, 1], 3, left).wait_recv()
        fourth = [to(buf.at[far], 7, twin)]
        fourth[0].start()
        for k, shift in ((4, 0), (5, n_tp - 2), (6, 2), (7, 4)):
            to(buf.at[lax.rem(twin + shift, n_tp)], k, twin).wait_recv()
        return first + second + third + fourth

    sent = tp_gather(x_buf, xs_sem, xr_sem)

    def pass_gate_up(i, c):
        s = lax.rem(me + n_fs - turn(i), n_fs)
        for a in (0, 1):
            z_copy(a, s, s).wait_recv()
            y_copy(a, q, s).start()
        return c

    lax.fori_loop(0, n_fs - 1, pass_gate_up, 0)

    def mate_gate_up(i, c):
        s = lax.rem(me + n_fs - turn(i), n_fs)
        for a in (0, 1):
            y_copy(a, other, s).wait_recv()
        return c

    lax.fori_loop(0, n_fs - 1, mate_gate_up, 0)
    outs = [
        pltpu.make_async_copy(og, og_out, out_sem.at[0]),
        pltpu.make_async_copy(ou, ou_out, out_sem.at[1]),
        pltpu.make_async_copy(od, od_out, out_sem.at[2]),
    ]
    outs[0].start()
    outs[1].start()

    width = og.shape[2]
    tile = x_buf.shape[2]

    def hidden(i, c):
        half, k = lax.div(i, 2), lax.rem(i, 2)
        acc = jnp.zeros((tile, 2 * width), F32)
        for f in range(n_tp):
            w = jnp.concatenate(
                [og[k, f * cols : (f + 1) * cols], ou[k, f * cols : (f + 1) * cols]], axis=1
            )
            acc += jnp.dot(x_buf[f, half], w, preferred_element_type=F32)
        g, u = acc[:, :width], acc[:, width:]
        act = g / (1.0 + jnp.exp(-g)) * u
        h_buf[t, k, pl.ds(pl.multiple_of(half * tile, tile), tile)] = act.astype(BF16)
        return c

    lax.fori_loop(0, 4, hidden, 0)

    eye = (
        lax.broadcasted_iota(jnp.int32, (per, 128), 0) == lax.broadcasted_iota(jnp.int32, (per, 128), 1)
    ).astype(F32)

    def columns(s, c):
        both = w_recv[s]
        for k in range(2):
            column = jnp.sum(eye * both[k : k + 1], axis=1, keepdims=True)
            w_rows[k, pl.ds(pl.multiple_of(s * per, per), per)] = jnp.broadcast_to(column, (per, 128))
        return c

    lax.fori_loop(0, n_fs, columns, 0)

    sent += tp_gather(h_buf, hs_sem, hr_sem)

    def pass_down(i, c):
        s = lax.rem(me + n_fs - turn(i), n_fs)
        z_copy(2, s, s).wait_recv()
        y_copy(2, q, s).start()
        return c

    lax.fori_loop(0, n_fs - 1, pass_down, 0)

    def mate_down(i, c):
        s = lax.rem(me + n_fs - turn(i), n_fs)
        y_copy(2, other, s).wait_recv()
        return c

    lax.fori_loop(0, n_fs - 1, mate_down, 0)
    outs[2].start()

    srcs = 4
    deep = srcs * per

    def outputs(i, c):
        rows = pl.ds(pl.multiple_of(i * deep, deep), deep)
        mix = jnp.zeros((deep, cols), F32)
        for k in range(2):
            acc = jnp.zeros((deep, cols), F32)
            for f in range(n_tp // 2):
                h = jnp.concatenate([h_buf[2 * f, k, rows], h_buf[2 * f + 1, k, rows]], axis=1)
                acc += jnp.dot(
                    h, od[k, 2 * f * width : 2 * (f + 1) * width], preferred_element_type=F32
                )
            w = w_rows[k, rows]
            mix += acc.astype(BF16).astype(F32) * jnp.concatenate([w] * (cols // 128), axis=1)
        mix = mix.astype(BF16)
        for b in range(srcs):
            for m in range(span):
                at = b * per + m * quarter
                spot = pl.ds(pl.multiple_of((i * srcs + b) * quarter, quarter), quarter)
                part[m, spot] = mix[at : at + quarter]
        return c

    lax.fori_loop(0, n_fs // srcs, outputs, 0)

    def part_copy(to_member, from_member):
        return remote(
            part.at[to_member], gathered.at[from_member], ps_sem.at[to_member], pr_sem.at[from_member],
            {"fs": base + to_member},
        )

    for i in range(1, span):
        part_copy(lax.rem(member + i, span), member).start()
    tot = part[member].astype(F32)
    for i in range(1, span):
        frm = lax.rem(member + span - i, span)
        part_copy(frm, frm).wait_recv()
        tot += gathered[frm].astype(F32)
    total[...] = tot.astype(BF16)

    def back_copy(j, s):
        return remote(
            total.at[pl.ds(pl.multiple_of(j * quarter, quarter), quarter)],
            final.at[pl.ds(pl.multiple_of(s * quarter, quarter), quarter)],
            fs_sem.at[j], fr_sem.at[s], {"fs": j},
        )

    def send_back(i, c):
        back_copy(lax.rem(me + turn(i), n_fs), me).start()
        return c

    lax.fori_loop(0, n_fs - 1, send_back, 0)
    here = pl.ds(pl.multiple_of(me * quarter, quarter), quarter)
    final[here] = total[here]

    def get_back(i, c):
        s = lax.rem(me + n_fs - turn(i), n_fs)
        back_copy(s, s).wait_recv()
        return c

    lax.fori_loop(0, n_fs - 1, get_back, 0)
    mix_ref[...] = jnp.dot(place, final[...], preferred_element_type=F32).astype(BF16)

    def drain(i, c):
        j = lax.rem(me + i, n_fs)
        tok_copy(j, me).wait_send()
        w_copy(j, me).wait_send()
        back_copy(j, me).wait_send()
        for a in range(3):
            z_copy(a, j, me).wait_send()
            y_copy(a, q, j).wait_send()
        return c

    lax.fori_loop(1, n_fs, drain, 0)
    for i in range(1, span):
        part_copy(lax.rem(member + i, span), member).wait_send()
    for copy in sent:
        copy.wait_send()
    for out in outs:
        out.wait()


def solution(mesh):
    n_fs, n_tp = mesh.shape["fs"], mesh.shape["tp"]

    def on_device(tokens, route_ids, route_weights, ffn_gain, gate_master, up_master, down_master):
        toks, d = tokens.shape
        experts, rows, width = gate_master.shape
        down_rows, cols = down_master.shape[1:]
        served = experts // n_fs
        span = GROUP_SIZE // served
        per = toks // (experts // GROUP_SIZE)
        all_rows = n_fs * per
        quarter = per // span
        dma = pltpu.SemaphoreType.DMA
        shape = jax.ShapeDtypeStruct
        vmem, hbm = pl.BlockSpec(memory_space=pltpu.VMEM), pl.BlockSpec(memory_space=pl.ANY)
        return tuple(
            pl.pallas_call(
                functools.partial(kernel, n_fs, n_tp, span),
                out_shape=(
                    shape((served, n_fs * rows, width), BF16),
                    shape((served, n_fs * rows, width), BF16),
                    shape((served, n_fs * down_rows, cols), BF16),
                    shape((toks, cols), BF16),
                ),
                in_specs=[vmem] * 4 + [hbm] * 3,
                out_specs=(hbm, hbm, hbm, vmem),
                scratch_shapes=[
                    pltpu.VMEM((n_fs, rows, width), F32),
                    pltpu.VMEM((n_fs, rows, width), F32),
                    pltpu.VMEM((n_fs, down_rows, cols), F32),
                    pltpu.VMEM((rows, width), F32),
                    pltpu.VMEM((rows, width), F32),
                    pltpu.VMEM((down_rows, cols), F32),
                    pltpu.VMEM((n_fs, rows, width), BF16),
                    pltpu.VMEM((n_fs, rows, width), BF16),
                    pltpu.VMEM((n_fs, down_rows, cols), BF16),
                    pltpu.VMEM((served, n_fs * rows, width), BF16),
                    pltpu.VMEM((served, n_fs * rows, width), BF16),
                    pltpu.VMEM((served, n_fs * down_rows, cols), BF16),
                    pltpu.VMEM((toks, cols), BF16),
                    pltpu.VMEM((n_fs, served, 128), F32),
                    pltpu.VMEM((n_tp, 2, all_rows // 2, cols), BF16),
                    pltpu.VMEM((n_fs, served, 128), F32),
                    pltpu.VMEM((n_tp, served, all_rows, width), BF16),
                    pltpu.VMEM((served, all_rows, 128), F32),
                    pltpu.VMEM((span, n_fs * quarter, cols), BF16),
                    pltpu.VMEM((span, n_fs * quarter, cols), BF16),
                    pltpu.VMEM((n_fs * quarter, cols), BF16),
                    pltpu.VMEM((n_fs * quarter, cols), BF16),
                    dma((6,)),
                    dma((3,)),
                    dma((3, n_fs)),
                    dma((3, n_fs)),
                    dma((3, n_fs)),
                    dma((3, n_fs)),
                    dma((2, n_fs)),
                    dma((2, n_fs)),
                    dma((8,)),
                    dma((8,)),
                    dma((8,)),
                    dma((8,)),
                    dma((span,)),
                    dma((span,)),
                    dma((n_fs,)),
                    dma((n_fs,)),
                ],
                compiler_params=pltpu.CompilerParams(
                    collective_id=0, has_side_effects=True, vmem_limit_bytes=56 * 1024 * 1024
                ),
                name="experts",
            )(
                tokens,
                route_ids,
                route_weights,
                ffn_gain.reshape(rows, 1),
                gate_master.reshape(n_fs, served, rows, width),
                up_master.reshape(n_fs, served, rows, width),
                down_master.reshape(n_fs, served, down_rows, cols),
            )
        )

    in_specs = (
        P(("grp", "fs"), None),
        P(("grp", "fs"), None),
        P(("grp", "fs"), None),
        P("fs"),
        P(None, "fs", "tp"),
        P(None, "fs", "tp"),
        P(None, "fs", "tp"),
    )
    out_specs = (
        P(("grp", "fs"), None, "tp"),
        P(("grp", "fs"), None, "tp"),
        P(("grp", "fs"), None, "tp"),
        P(("grp", "fs"), "tp"),
    )
    return jax.shard_map(
        on_device, mesh=mesh, in_specs=in_specs, out_specs=out_specs, check_vma=False
    )
```

time: 302 us -> 179 us (0.59)
  waiting for transfers between devices: 198 us -> 0 us
  Pallas kernels: 0 us -> 167 us
  starting transfers between devices: 51.2 us -> 0 us
  between operations: 14.1 us -> 0.66 us
  local copies, waits for them, and re-layouts: 21.2 us -> 9.36 us
  other arithmetic: 11.2 us -> 0 us
  matrix products: 5.54 us -> 0 us
    pallas_call x0 -> x1, Pallas kernels: none -> 167 us  [on_device(): pl.pallas_call(functools.partial(kernel, n_fs, n_tp, span), out_shape=(sh...]
    all_to_all x4 -> x0, waiting for transfers between devices: 117 us -> none  [the longest x1 51.4 us: in_one_piece(): lax.all_to_all(both, axis, split_axis=split_dim, concat_axis=concat_dim,...]
    all_gather x4 -> x0, waiting for transfers between devices: 80.4 us -> none  [gather_in_order(): blocks = lax.all_gather(blocks, axes[k], axis=0, tiled=True)]
    all_to_all x4 -> x0, starting transfers between devices: 50.8 us -> none  [the longest x1 24 us: on_device(): lax.all_to_all(fill_slots(own_cols, targets, experts, capacity), 'fs', sp...]
    transpose x2 -> x0, local copies, waits for them, and re-layouts: 6.93 us -> none  [gather_in_order(): blocks.transpose(*turned, *range(len(turns), blocks.ndim))]
    unnamed x20 -> x12, local copies, waits for them, and re-layouts: 1.1 us -> 7.97 us
    convert_element_type x5 -> x0, other arithmetic: 6.55 us -> none  [the longest x1 2.71 us: on_device(): down_local = down_master.astype(jnp.bfloat16)]
    dot_general x3 -> x0, matrix products: 5.54 us -> none  [the longest x1 2.31 us: on_device(): jnp.einsum('erf,efd->erd', gathered_by_axis(hidden, TP, (0, 1), 2), down_...]
  transfers between devices with their start and end apart: 8 -> 0, of which waited for: 7 -> 0; matrix products, arithmetic and copies ran while one was open for 5% -> 0% of each run, Pallas kernels for 0% -> 0%
where the time goes in v1:
time: 179 us; the launch traced here: 177 us
  Pallas kernels  167 us (93%)
  local copies, waits for them, and re-layouts  9.36 us (5%)
    pallas_call x1, Pallas kernels, on_device(): pl.pallas_call(functools.partial(kernel, n_fs, n_tp, span), out_shape=(sh...  167 us
    unnamed x12, local copies, waits for them, and re-layouts  7.97 us

profile of v1, /device:TPU:34, one launch (start us, length us, event | category | flops | bytes accessed | tf_op | source)
XLA Modules:
  0.0 176.9 jit_solution(17132371459348365318)
XLA Ops:
  0.6 1.4 copy.13.gain_ref
  2.0 1.5 copy.11.ids_ref
  3.5 1.5 copy.12.rw_ref
  5.0 166.9 %experts.1 = (bf16[2,2048,128]{2,1,0:T(8,128)(2,1)}, bf16[2,2048,128]{2,1,0:T(8,128)(2,1)}, bf16[2,1024,256]{2,1,0:T(8,128)(2,1)}, bf16[256,256]{1,0:T(8,128)(2,1)}) custom-call(bf16[256,2048]{1,0:T(8,128)(2,1)} %tok_ref.1, s32[256,2]{1,0:T(8,128)} %copy.11.ids_ref, f32[256,2]{1,0:T(8,128)} %copy.12.rw_ref, f32[128,1]{1,0:T(8,128)} %copy.13.gain_ref, ...), custom_call_target="tpu_custom_call" | custom-call | tf_op jit(solution)/shard_map/experts/pallas_call | solution.py:386
  171.8 0.0 copy-start.1
  171.8 0.0 copy-start
  171.9 2.4 %copy.18 = bf16[2,2048,128]{2,1,0:T(8,128)(2,1)} copy(bf16[2,2048,128]{2,1,0:T(8,128)(2,1)} %get-tuple-element.8) | data formatting | bytes 2097152
  174.3 0.0 copy-done.1
  174.3 0.0 copy-start.2
  174.3 1.0 copy.19
  175.2 0.0 copy-done
  175.2 1.0 copy.20
  176.2 0.0 copy-done.2
  176.2 0.7 copy.21
Async XLA Ops:
  171.8 2.4 %copy-start.1 = (bf16[2,2048,128]{2,1,0:T(8,128)(2,1)S(1)}, bf16[2,2048,128]{2,1,0:T(8,128)(2,1)}, u32[]{:S(2)}) copy-start(bf16[2,2048,128]{2,1,0:T(8,128)(2,1)} %get-tuple-element.9) | copy-start | bytes 3145732
  171.8 3.4 %copy-start = (bf16[2,1024,256]{2,1,0:T(8,128)(2,1)S(1)}, bf16[2,1024,256]{2,1,0:T(8,128)(2,1)}, u32[]{:S(2)}) copy-start(bf16[2,1024,256]{2,1,0:T(8,128)(2,1)} %get-tuple-element.10) | copy-start | bytes 3145732
  174.3 1.9 %copy-start.2 = (bf16[256,256]{1,0:T(8,128)(2,1)S(1)}, bf16[256,256]{1,0:T(8,128)(2,1)}, u32[]{:S(2)}) copy-start(bf16[256,256]{1,0:T(8,128)(2,1)} %get-tuple-element.11) | copy-start | bytes 393220

commit v2 on v1

v2 whole, which is shorter than its diff:
```python
import functools

import jax
import jax.numpy as jnp
from jax import lax
from jax.experimental import pallas as pl
from jax.experimental.pallas import tpu as pltpu
from jax.sharding import PartitionSpec as P

GROUP_SIZE = 8
MESH = pl.DeviceIdType.MESH
BF16 = jnp.bfloat16
F32 = jnp.float32
PASS_GATE_UP = (6, 8)
PASS_DOWN = (5, 9)


def remote(src, dst, send, recv, where):
    return pltpu.make_async_remote_copy(
        src_ref=src, dst_ref=dst, send_sem=send, recv_sem=recv, device_id=where, device_id_type=MESH
    )


def kernel(
    n_fs, n_tp, span,
    tok_ref, ids_ref, rw_ref, gain_ref, gm_ref, um_ref, dm_ref,
    og, ou, od, mix_ref,
    g_in, u_in, d_in, g_own, u_own, d_own, g_send, u_send, d_send,
    s_buf, w_send, x_buf, w_recv, h_buf, w_rows, pick, spread, part, gathered, total, final,
    load_sem, z_send, z_recv, y_send, y_recv, w_sems, t_send, t_recv,
    xs_sem, xr_sem, hs_sem, hr_sem, ps_sem, pr_sem, fs_sem, fr_sem,
):
    grp, me, t = lax.axis_index("grp"), lax.axis_index("fs"), lax.axis_index("tp")
    q = lax.rem(grp, 2)
    other = 1 - q
    mate = grp + 1 - 2 * q
    right, left = lax.rem(t + 2, n_tp), lax.rem(t + n_tp - 2, n_tp)
    far = lax.rem(t + 4, n_tp)
    twin = t + 1 - 2 * lax.rem(t, 2)
    member = lax.rem(me, span)
    base = me - member
    groups = n_fs // span
    gid = lax.div(me, span)
    gnext, gprev, gopp = (lax.rem(gid + k, groups) for k in (1, groups - 1, groups // 2))
    toks = tok_ref.shape[0]
    cols = s_buf.shape[1]
    per = s_buf.shape[0] // groups
    quarter = per // span
    slots = per // 2

    def turn(i):
        half = lax.div(i, 2)
        odd = lax.rem(i, 2)
        return half + 1 + odd * (n_fs - 2 * half - 2)

    barrier = pltpu.get_barrier_semaphore()

    def greet(i, c):
        pl.semaphore_signal(
            barrier, inc=1, device_id={"fs": lax.rem(me + i, n_fs)}, device_id_type=MESH
        )
        return c

    lax.fori_loop(1, n_fs, greet, 0)
    pl.semaphore_signal(barrier, inc=1, device_id={"grp": mate}, device_id_type=MESH)
    for peer in (right, left, twin):
        pl.semaphore_signal(barrier, inc=1, device_id={"tp": peer}, device_id_type=MESH)

    loads = [
        pltpu.make_async_copy(gm_ref.at[:, q], g_in, load_sem.at[0]),
        pltpu.make_async_copy(um_ref.at[:, q], u_in, load_sem.at[1]),
        pltpu.make_async_copy(dm_ref.at[:, q], d_in, load_sem.at[2]),
        pltpu.make_async_copy(gm_ref.at[me, other], g_own, load_sem.at[3]),
        pltpu.make_async_copy(um_ref.at[me, other], u_own, load_sem.at[4]),
        pltpu.make_async_copy(dm_ref.at[me, other], d_own, load_sem.at[5]),
    ]
    for load in loads:
        load.start()

    ids = ids_ref[...]
    first, second = ids[0:1], ids[1:2]
    group = lax.shift_right_logical(first, GROUP_SIZE.bit_length() - 1)
    group_hot = (group == lax.broadcasted_iota(jnp.int32, (8, toks), 0)).astype(F32)
    row = lax.broadcasted_iota(jnp.int32, (toks, toks), 0)
    col = lax.broadcasted_iota(jnp.int32, (toks, toks), 1)
    counts = jnp.dot(
        group_hot.astype(BF16), (row < col).astype(BF16), preferred_element_type=F32
    )
    rank = jnp.sum(counts * group_hot, axis=0, keepdims=True)
    target = group.astype(F32) * per + rank
    place = (target == row.astype(F32)).astype(BF16)
    tok = tok_ref[...].astype(F32)
    scale = lax.rsqrt(jnp.mean(tok * tok, axis=1, keepdims=True) + 1e-06)
    own = tok_ref[:, pl.ds(pl.multiple_of(t * cols, cols), cols)].astype(F32)
    normed = (own * scale).astype(BF16)
    s_buf[...] = jnp.dot(place, normed, preferred_element_type=F32).astype(BF16)
    rw = rw_ref[...]
    expert = lax.broadcasted_iota(jnp.int32, (2 * n_fs, toks), 0)
    by_expert = jnp.where(first == expert, rw[0:1], 0.0) + jnp.where(second == expert, rw[1:2], 0.0)
    rank_hot = (rank == lax.broadcasted_iota(jnp.int32, (128, toks), 0).astype(F32)).astype(F32)
    w_all = lax.dot_general(
        by_expert, rank_hot, (((1,), (1,)), ((), ())),
        preferred_element_type=F32, precision=lax.Precision.HIGHEST,
    )
    for j in range(n_fs):
        w_send[j] = w_all[2 * j : 2 * j + 2]

    pl.semaphore_wait(barrier, n_fs - 1 + 4)

    x_half = x_buf.shape[2] // per

    def rows_at(s):
        return x_buf.at[
            t, lax.div(s, x_half), pl.ds(pl.multiple_of(lax.rem(s, x_half) * per, per), per)
        ]

    def row_copy(j, s):
        begin = pl.multiple_of(lax.div(j, span) * per, per)
        return remote(
            s_buf.at[pl.ds(begin, per)], rows_at(s), t_send.at[j], t_recv.at[s], {"fs": j}
        )

    def w_copy(j, s):
        return remote(w_send.at[j], w_recv.at[s], w_sems.at[0, j], w_sems.at[1, s], {"fs": j})

    def dispatch(i, c):
        j = lax.rem(me + turn(i), n_fs)
        row_copy(j, me).start()
        w_copy(j, me).start()
        return c

    lax.fori_loop(0, n_fs - 1, dispatch, 0)

    gain_row = gain_ref[...]
    side = gain_row.shape[1]
    diagonal = lax.broadcasted_iota(jnp.int32, (side, side), 0) == lax.broadcasted_iota(
        jnp.int32, (side, side), 1
    )
    gain = jnp.broadcast_to(
        jnp.sum(jnp.where(diagonal, gain_row, 0.0), axis=1, keepdims=True), g_own.shape
    )
    gate_rows, down_rows = g_own.shape[0], d_own.shape[0]

    def gate_at(buf, e, s):
        return buf.at[e, pl.ds(pl.multiple_of(s * gate_rows, gate_rows), gate_rows)]

    def down_at(buf, e, s):
        return buf.at[e, pl.ds(pl.multiple_of(s * down_rows, down_rows), down_rows)]

    def z_copy(a, j, s):
        src = (g_send, u_send, d_send)[a].at[j]
        dst = (gate_at(og, q, s), gate_at(ou, q, s), down_at(od, q, s))[a]
        return remote(src, dst, z_send.at[a, j], z_recv.at[a, s], {"fs": j})

    def y_copy(a, e, s):
        spot = (gate_at(og, e, s), gate_at(ou, e, s), down_at(od, e, s))[a]
        return remote(spot, spot, y_send.at[a, s], y_recv.at[a, s], {"grp": mate})

    def send_gate_up(i, c):
        j = lax.rem(me + turn(i), n_fs)
        g_send[j] = (g_in[j] * gain).astype(BF16)
        u_send[j] = (u_in[j] * gain).astype(BF16)
        z_copy(0, j, me).start()
        z_copy(1, j, me).start()
        return c

    def send_down(i, c):
        j = lax.rem(me + turn(i), n_fs)
        d_send[j] = d_in[j].astype(BF16)
        z_copy(2, j, me).start()
        return c

    def pass_on(arrays, begin, end):
        def one(i, c):
            s = lax.rem(me + n_fs - turn(i), n_fs)
            for a in arrays:
                z_copy(a, s, s).wait_recv()
                y_copy(a, q, s).start()
            return c

        lax.fori_loop(begin, end, one, 0)

    def from_mate(arrays):
        def one(i, c):
            s = lax.rem(me + n_fs - turn(i), n_fs)
            for a in arrays:
                y_copy(a, other, s).wait_recv()
            return c

        lax.fori_loop(0, n_fs - 1, one, 0)

    last = n_fs - 1
    loads[0].wait()
    loads[1].wait()
    lax.fori_loop(0, last, send_gate_up, 0)
    for load in loads[2:]:
        load.wait()
    lax.fori_loop(0, last, send_down, 0)
    own_rows = s_buf[pl.ds(pl.multiple_of(gid * per, per), per)]
    x_buf[t, lax.div(me, x_half), pl.ds(pl.multiple_of(lax.rem(me, x_half) * per, per), per)] = own_rows
    w_recv[me] = w_send[me]

    def tp_gather(buf, send, recv, between):
        def to(block, k, peer):
            return remote(block, block, send.at[k], recv.at[k], {"tp": peer})

        one = [to(buf.at[t], 0, right), to(buf.at[t], 1, left), to(buf.at[t], 4, twin)]
        for copy in one:
            copy.start()
        between[0]()
        to(buf.at[left], 0, right).wait_recv()
        two = [to(buf.at[left, 0], 2, right), to(buf.at[left], 5, twin)]
        for copy in two:
            copy.start()
        to(buf.at[right], 1, left).wait_recv()
        three = [to(buf.at[right, 1], 3, left), to(buf.at[right], 6, twin)]
        for copy in three:
            copy.start()
        between[1]()
        to(buf.at[far, 0], 2, right).wait_recv()
        to(buf.at[far, 1], 3, left).wait_recv()
        four = [to(buf.at[far], 7, twin)]
        four[0].start()
        between[2]()
        for k, shift in ((4, 0), (5, n_tp - 2), (6, 2), (7, 4)):
            to(buf.at[lax.rem(twin + shift, n_tp)], k, twin).wait_recv()
        return one + two + three + four

    eye = (
        lax.broadcasted_iota(jnp.int32, (per, 128), 0) == lax.broadcasted_iota(jnp.int32, (per, 128), 1)
    ).astype(F32)
    before = (
        lax.broadcasted_iota(jnp.int32, (128, 128), 0) < lax.broadcasted_iota(jnp.int32, (128, 128), 1)
    ).astype(BF16)
    slot_down = lax.broadcasted_iota(jnp.int32, (slots, 128), 0).astype(F32)
    slot_along = lax.broadcasted_iota(jnp.int32, (per, 128), 1).astype(F32)

    def index_rows():
        def one(s, c):
            both = w_recv[s]
            used = both > 0.0
            at = jnp.dot(used.astype(BF16), before, preferred_element_type=F32)
            at = jnp.where(used, at, -1.0)
            for k in range(2):
                pick[2 * s + k] = (at[k : k + 1] == slot_down).astype(BF16)
                column = jnp.sum(eye * both[k : k + 1], axis=1, keepdims=True)
                w_rows[k, pl.ds(pl.multiple_of(s * per, per), per)] = jnp.broadcast_to(column, (per, 128))
                at_col = jnp.sum(eye * at[k : k + 1], axis=1, keepdims=True)
                spread[2 * s + k] = (at_col == slot_along).astype(BF16)
            return c

        lax.fori_loop(0, n_fs, one, 0)

    def own_blocks():
        gate_spot = pl.ds(pl.multiple_of(me * gate_rows, gate_rows), gate_rows)
        down_spot = pl.ds(pl.multiple_of(me * down_rows, down_rows), down_rows)
        og[q, gate_spot] = (g_in[me] * gain).astype(BF16)
        ou[q, gate_spot] = (u_in[me] * gain).astype(BF16)
        od[q, down_spot] = d_in[me].astype(BF16)
        og[other, gate_spot] = (g_own[...] * gain).astype(BF16)
        ou[other, gate_spot] = (u_own[...] * gain).astype(BF16)
        od[other, down_spot] = d_own[...].astype(BF16)

    def rows_in(i, c):
        s = lax.rem(me + n_fs - turn(i), n_fs)
        row_copy(s, s).wait_recv()
        w_copy(s, s).wait_recv()
        return c

    own_blocks()
    lax.fori_loop(0, last, rows_in, 0)

    def while_x():
        index_rows()
        pass_on((0, 1), 0, PASS_GATE_UP[0])

    sent = tp_gather(
        x_buf, xs_sem, xr_sem,
        (
            while_x,
            lambda: pass_on((0, 1), PASS_GATE_UP[0], PASS_GATE_UP[1]),
            lambda: pass_on((0, 1), PASS_GATE_UP[1], last),
        ),
    )
    from_mate((0, 1))

    width = og.shape[2]
    tile = x_buf.shape[2]

    def hidden(i, c):
        half, k = lax.div(i, 2), lax.rem(i, 2)
        acc = jnp.zeros((tile, 2 * width), F32)
        for f in range(n_tp):
            w = jnp.concatenate(
                [og[k, f * cols : (f + 1) * cols], ou[k, f * cols : (f + 1) * cols]], axis=1
            )
            acc += jnp.dot(x_buf[f, half], w, preferred_element_type=F32)
        g, u = acc[:, :width], acc[:, width:]
        act = (g / (1.0 + jnp.exp(-g)) * u).astype(BF16)
        for b in range(tile // per):
            s = half * x_half + b
            rows = jnp.dot(
                pick[2 * s + k][:, :per], act[b * per : (b + 1) * per], preferred_element_type=F32
            )
            h_buf[t, k, pl.ds(pl.multiple_of(s * slots, slots), slots)] = rows.astype(BF16)
        return c

    lax.fori_loop(0, 4, hidden, 0)
    sent += tp_gather(
        h_buf, hs_sem, hr_sem,
        (
            lambda: pass_on((2,), 0, PASS_DOWN[0]),
            lambda: pass_on((2,), PASS_DOWN[0], PASS_DOWN[1]),
            lambda: pass_on((2,), PASS_DOWN[1], last),
        ),
    )
    from_mate((2,))

    deep = span * slots

    def outputs(sg):
        rows = pl.ds(pl.multiple_of(sg * deep, deep), deep)
        outs = []
        for k in range(2):
            acc = jnp.zeros((deep, cols), F32)
            for f in range(n_tp // 2):
                h = jnp.concatenate([h_buf[2 * f, k, rows], h_buf[2 * f + 1, k, rows]], axis=1)
                acc += jnp.dot(
                    h, od[k, 2 * f * width : 2 * (f + 1) * width], preferred_element_type=F32
                )
            outs.append(acc.astype(BF16))
        for b in range(span):
            s = sg * span + b
            mix = jnp.zeros((per, cols), F32)
            for k in range(2):
                full = jnp.dot(
                    spread[2 * s + k][:, :slots], outs[k][b * slots : (b + 1) * slots],
                    preferred_element_type=F32,
                )
                w = w_rows[k, pl.ds(pl.multiple_of(s * per, per), per)]
                mix += full * jnp.concatenate([w] * (cols // 128), axis=1)
            mix = mix.astype(BF16)
            for m in range(span):
                part[sg, m, b * quarter : (b + 1) * quarter] = mix[m * quarter : (m + 1) * quarter]

    def part_copy(sg, to_member, from_member):
        return remote(
            part.at[sg, to_member], gathered.at[sg, from_member],
            ps_sem.at[sg, to_member], pr_sem.at[sg, from_member], {"fs": base + to_member},
        )

    def back_copy(sg, b, s):
        return remote(
            total.at[sg, b * quarter : (b + 1) * quarter],
            final.at[pl.ds(pl.multiple_of(s * quarter, quarter), quarter)],
            fs_sem.at[sg, b], fr_sem.at[s], {"fs": sg * span + b},
        )

    order = (gopp, gnext, gprev, gid)
    for sg in order:
        outputs(sg)
        for i in range(1, span):
            part_copy(sg, lax.rem(member + i, span), member).start()
    for sg in order:
        tot = part[sg, member].astype(F32)
        for i in range(1, span):
            frm = lax.rem(member + span - i, span)
            part_copy(sg, frm, frm).wait_recv()
            tot += gathered[sg, frm].astype(F32)
        total[sg] = tot.astype(BF16)
        for b in range(span):
            if sg is not gid:
                back_copy(sg, b, me).start()
            else:

                @pl.when(member != b)
                def _():
                    back_copy(sg, b, me).start()

    here = pl.ds(pl.multiple_of(me * quarter, quarter), quarter)
    final[here] = total[gid, pl.ds(pl.multiple_of(member * quarter, quarter), quarter)]

    def get_back(i, c):
        s = lax.rem(me + n_fs - turn(i), n_fs)
        remote(final.at[here], final.at[here], fr_sem.at[s], fr_sem.at[s], {"fs": s}).wait_recv()
        return c

    lax.fori_loop(0, last, get_back, 0)
    mix_ref[...] = lax.dot_general(
        place, final[...], (((0,), (0,)), ((), ())), preferred_element_type=F32
    ).astype(BF16)

    def drain(i, c):
        j = lax.rem(me + i, n_fs)
        row_copy(j, me).wait_send()
        w_copy(j, me).wait_send()
        for a in range(3):
            z_copy(a, j, me).wait_send()
            y_copy(a, q, j).wait_send()
        return c

    lax.fori_loop(1, n_fs, drain, 0)
    for sg in order:
        for i in range(1, span):
            part_copy(sg, lax.rem(member + i, span), member).wait_send()
        for b in range(span):
            if sg is not gid:
                back_copy(sg, b, me).wait_send()
            else:

                @pl.when(member != b)
                def _():
                    back_copy(sg, b, me).wait_send()

    for copy in sent:
        copy.wait_send()


def write_out(*refs):
    half = len(refs) // 2
    ins, outs, sems = refs[:half], refs[half : 2 * half], refs[2 * half]
    copies = [pltpu.make_async_copy(a, b, sems.at[i]) for i, (a, b) in enumerate(zip(ins, outs))]
    for copy in copies:
        copy.start()
    for copy in copies:
        copy.wait()


def solution(mesh):
    n_fs, n_tp = mesh.shape["fs"], mesh.shape["tp"]

    def on_device(tokens, route_ids, route_weights, ffn_gain, gate_master, up_master, down_master):
        toks, d = tokens.shape
        experts, rows, width = gate_master.shape
        down_rows, cols = down_master.shape[1:]
        served = experts // n_fs
        span = GROUP_SIZE // served
        per = toks // (experts // GROUP_SIZE)
        all_rows = n_fs * per
        quarter = per // span
        dma = pltpu.SemaphoreType.DMA
        shape = jax.ShapeDtypeStruct
        vmem, hbm = pl.BlockSpec(memory_space=pltpu.VMEM), pl.BlockSpec(memory_space=pl.ANY)
        groups = n_fs // span
        out_shape = (
            shape((served, n_fs * rows, width), BF16),
            shape((served, n_fs * rows, width), BF16),
            shape((served, n_fs * down_rows, cols), BF16),
            shape((toks, cols), BF16),
        )
        results = pl.pallas_call(
            functools.partial(kernel, n_fs, n_tp, span),
            out_shape=out_shape,
            in_specs=[vmem] * 4 + [hbm] * 3,
            out_specs=(vmem,) * 4,
            scratch_shapes=[
                pltpu.VMEM((n_fs, rows, width), F32),
                pltpu.VMEM((n_fs, rows, width), F32),
                pltpu.VMEM((n_fs, down_rows, cols), F32),
                pltpu.VMEM((rows, width), F32),
                pltpu.VMEM((rows, width), F32),
                pltpu.VMEM((down_rows, cols), F32),
                pltpu.VMEM((n_fs, rows, width), BF16),
                pltpu.VMEM((n_fs, rows, width), BF16),
                pltpu.VMEM((n_fs, down_rows, cols), BF16),
                pltpu.VMEM((toks, cols), BF16),
                pltpu.VMEM((n_fs, served, 128), F32),
                pltpu.VMEM((n_tp, 2, all_rows // 2, cols), BF16),
                pltpu.VMEM((n_fs, served, 128), F32),
                pltpu.VMEM((n_tp, served, all_rows // 2, width), BF16),
                pltpu.VMEM((served, all_rows, 128), F32),
                pltpu.VMEM((n_fs * served, per // 2, 128), BF16),
                pltpu.VMEM((n_fs * served, per, 128), BF16),
                pltpu.VMEM((groups, span, span * quarter, cols), BF16),
                pltpu.VMEM((groups, span, span * quarter, cols), BF16),
                pltpu.VMEM((groups, span * quarter, cols), BF16),
                pltpu.VMEM((n_fs * quarter, cols), BF16),
                dma((6,)),
                dma((3, n_fs)),
                dma((3, n_fs)),
                dma((3, n_fs)),
                dma((3, n_fs)),
                dma((2, n_fs)),
                dma((n_fs,)),
                dma((n_fs,)),
                dma((8,)),
                dma((8,)),
                dma((8,)),
                dma((8,)),
                dma((groups, span)),
                dma((groups, span)),
                dma((groups, span)),
                dma((n_fs,)),
            ],
            compiler_params=pltpu.CompilerParams(
                collective_id=0, has_side_effects=True, vmem_limit_bytes=50 * 1024 * 1024
            ),
            name="experts",
        )(
            tokens,
            route_ids.T,
            route_weights.T,
            ffn_gain.reshape(1, rows),
            gate_master.reshape(n_fs, served, rows, width),
            up_master.reshape(n_fs, served, rows, width),
            down_master.reshape(n_fs, served, down_rows, cols),
        )
        return tuple(
            pl.pallas_call(
                write_out,
                out_shape=out_shape,
                in_specs=[vmem] * 4,
                out_specs=(hbm,) * 4,
                scratch_shapes=[dma((4,))],
                compiler_params=pltpu.CompilerParams(vmem_limit_bytes=8 * 1024 * 1024),
                name="write_out",
            )(*results)
        )

    in_specs = (
        P(("grp", "fs"), None),
        P(("grp", "fs"), None),
        P(("grp", "fs"), None),
        P("fs"),
        P(None, "fs", "tp"),
        P(None, "fs", "tp"),
        P(None, "fs", "tp"),
    )
    out_specs = (
        P(("grp", "fs"), None, "tp"),
        P(("grp", "fs"), None, "tp"),
        P(("grp", "fs"), None, "tp"),
        P(("grp", "fs"), "tp"),
    )
    return jax.shard_map(
        on_device, mesh=mesh, in_specs=in_specs, out_specs=out_specs, check_vma=False
    )
```

time: 179 us -> 152 us (0.85)
  Pallas kernels: 167 us -> 148 us
  local copies, waits for them, and re-layouts: 9.36 us -> 2.01 us
    pallas_call x1 -> x2, Pallas kernels: 167 us -> 148 us  [the longest x1 147 us: on_device(): pl.pallas_call(functools.partial(kernel, n_fs, n_tp, span), out_shape=out...]
    unnamed x12 -> x6, local copies, waits for them, and re-layouts: 7.97 us -> 2.01 us
where the time goes in v2:
time: 152 us; the launch traced here: 151 us
  Pallas kernels  148 us (97%)
  local copies, waits for them, and re-layouts  2.01 us (1%)
    pallas_call x1, Pallas kernels, on_device(): pl.pallas_call(functools.partial(kernel, n_fs, n_tp, span), out_shape=out...  147 us

profile of v2, /device:TPU:34, one launch (start us, length us, event | category | flops | bytes accessed | tf_op | source)
XLA Modules:
  0.0 150.9 jit_solution(10535333708037379969)
XLA Ops:
  0.6 0.0 copy-start
  0.6 0.7 copy-done
  1.3 0.0 copy-start.1
  1.3 0.7 copy-done.1
  2.0 0.0 copy-start.2
  2.0 0.7 copy-done.2
  2.7 146.5 %experts.1 = (bf16[2,2048,128]{2,1,0:T(8,128)(2,1)S(1)}, bf16[2,2048,128]{2,1,0:T(8,128)(2,1)S(1)}, bf16[2,1024,256]{2,1,0:T(8,128)(2,1)S(1)}, bf16[256,256]{1,0:T(8,128)(2,1)S(1)}) custom-call(bf16[256,2048]{1,0:T(8,128)(2,1)} %tok_ref.1, s32[2,256]{1,0:T(2,128)S(1)} %bitcast.6, f32[2,256]{1,0:T(2,128)S(1)} %bitcast.7, f32[1,128]{1,0:T(1,128)S(1)} %bitcast.8, ...), custom_call_target="tpu_custom_call" | custom-call | tf_op jit(solution)/shard_map/experts/pallas_call | solution.py:451
  149.2 1.7 %write_out.1 = (bf16[2,2048,128]{2,1,0:T(8,128)(2,1)}, bf16[2,2048,128]{2,1,0:T(8,128)(2,1)}, bf16[2,1024,256]{2,1,0:T(8,128)(2,1)}, bf16[256,256]{1,0:T(8,128)(2,1)}) custom-call(bf16[2,2048,128]{2,1,0:T(8,128)(2,1)S(1)} %get-tuple-element.8.refs_0_, bf16[2,2048,128]{2,1,0:T(8,128)(2,1)S(1)} %get-tuple-element.9.refs_1_, ...), custom_call_target="tpu_custom_call" | custom-call | tf_op jit(solution)/shard_map/write_out/pallas_call | solution.py:509
Async XLA Ops:
  0.6 0.7 copy-start
  1.3 0.7 copy-start.1
  2.0 0.7 copy-start.2

commit v3 on v2

--- a/solution.py
+++ b/solution.py
@@ -23,8 +23,9 @@
 
 def kernel(
     n_fs, n_tp, span,
-    tok_ref, ids_ref, rw_ref, gain_ref, gm_ref, um_ref, dm_ref,
+    tok_hbm, ids_hbm, rw_hbm, gain_hbm, gm_ref, um_ref, dm_ref,
     og, ou, od, mix_ref,
+    tok_ref, ids_ref, rw_ref, gain_ref, own_part, own_in,
     g_in, u_in, d_in, g_own, u_own, d_own, g_send, u_send, d_send,
     s_buf, w_send, x_buf, w_recv, h_buf, w_rows, pick, spread, part, gathered, total, final,
     load_sem, z_send, z_recv, y_send, y_recv, w_sems, t_send, t_recv,
@@ -74,9 +75,17 @@
         pltpu.make_async_copy(um_ref.at[me, other], u_own, load_sem.at[4]),
         pltpu.make_async_copy(dm_ref.at[me, other], d_own, load_sem.at[5]),
     ]
-    for load in loads:
+    small = [
+        pltpu.make_async_copy(a, b, load_sem.at[6 + i])
+        for i, (a, b) in enumerate(
+            ((ids_hbm, ids_ref), (rw_hbm, rw_ref), (gain_hbm, gain_ref), (tok_hbm, tok_ref))
+        )
+    ]
+    for load in small + loads:
         load.start()
 
+    for load in small:
+        load.wait()
     ids = ids_ref[...]
     first, second = ids[0:1], ids[1:2]
     group = lax.shift_right_logical(first, GROUP_SIZE.bit_length() - 1)
@@ -340,12 +349,17 @@
                 w = w_rows[k, pl.ds(pl.multiple_of(s * per, per), per)]
                 mix += full * jnp.concatenate([w] * (cols // 128), axis=1)
             mix = mix.astype(BF16)
+            if sg is gid:
+                own_part[b] = mix
+                continue
             for m in range(span):
                 part[sg, m, b * quarter : (b + 1) * quarter] = mix[m * quarter : (m + 1) * quarter]
 
     def part_copy(sg, to_member, from_member):
+        direct = sg is gid
         return remote(
-            part.at[sg, to_member], gathered.at[sg, from_member],
+            own_part.at[to_member] if direct else part.at[sg, to_member],
+            own_in.at[from_member] if direct else gathered.at[sg, from_member],
             ps_sem.at[sg, to_member], pr_sem.at[sg, from_member], {"fs": base + to_member},
         )
 
@@ -356,12 +370,13 @@
             fs_sem.at[sg, b], fr_sem.at[s], {"fs": sg * span + b},
         )
 
-    order = (gopp, gnext, gprev, gid)
-    for sg in order:
+    abroad = (gopp, gnext, gprev)
+    for sg in abroad:
         outputs(sg)
         for i in range(1, span):
             part_copy(sg, lax.rem(member + i, span), member).start()
-    for sg in order:
+    outputs(gid)
+    for sg in abroad:
         tot = part[sg, member].astype(F32)
         for i in range(1, span):
             frm = lax.rem(member + span - i, span)
@@ -369,23 +384,25 @@
             tot += gathered[sg, frm].astype(F32)
         total[sg] = tot.astype(BF16)
         for b in range(span):
-            if sg is not gid:
-                back_copy(sg, b, me).start()
-            else:
-
-                @pl.when(member != b)
-                def _():
-                    back_copy(sg, b, me).start()
-
-    here = pl.ds(pl.multiple_of(me * quarter, quarter), quarter)
-    final[here] = total[gid, pl.ds(pl.multiple_of(member * quarter, quarter), quarter)]
+            back_copy(sg, b, me).start()
+        if sg is gopp:
+            for i in range(1, span):
+                part_copy(gid, lax.rem(member + i, span), member).start()
+
+    tot = own_part[member].astype(F32)
+    for i in range(1, span):
+        frm = lax.rem(member + span - i, span)
+        part_copy(gid, frm, frm).wait_recv()
+        tot += own_in[frm].astype(F32)
+    final[pl.ds(pl.multiple_of(gid * per, per), per)] = tot.astype(BF16)
 
     def get_back(i, c):
-        s = lax.rem(me + n_fs - turn(i), n_fs)
-        remote(final.at[here], final.at[here], fr_sem.at[s], fr_sem.at[s], {"fs": s}).wait_recv()
-        return c
-
-    lax.fori_loop(0, last, get_back, 0)
+        s = lax.rem(base + span + i, n_fs)
+        spot = pl.ds(pl.multiple_of(s * quarter, quarter), quarter)
+        remote(final.at[spot], final.at[spot], fr_sem.at[s], fr_sem.at[s], {"fs": s}).wait_recv()
+        return c
+
+    lax.fori_loop(0, n_fs - span, get_back, 0)
     mix_ref[...] = lax.dot_general(
         place, final[...], (((0,), (0,)), ((), ())), preferred_element_type=F32
     ).astype(BF16)
@@ -400,17 +417,12 @@
         return c
 
     lax.fori_loop(1, n_fs, drain, 0)
-    for sg in order:
+    for sg in abroad + (gid,):
         for i in range(1, span):
             part_copy(sg, lax.rem(member + i, span), member).wait_send()
+    for sg in abroad:
         for b in range(span):
-            if sg is not gid:
-                back_copy(sg, b, me).wait_send()
-            else:
-
-                @pl.when(member != b)
-                def _():
-                    back_copy(sg, b, me).wait_send()
+            back_copy(sg, b, me).wait_send()
 
     for copy in sent:
         copy.wait_send()
@@ -451,9 +463,15 @@
         results = pl.pallas_call(
             functools.partial(kernel, n_fs, n_tp, span),
             out_shape=out_shape,
-            in_specs=[vmem] * 4 + [hbm] * 3,
+            in_specs=[hbm] * 7,
             out_specs=(vmem,) * 4,
             scratch_shapes=[
+                pltpu.VMEM((toks, d), BF16),
+                pltpu.VMEM((2, toks), jnp.int32),
+                pltpu.VMEM((2, toks), F32),
+                pltpu.VMEM((1, rows), F32),
+                pltpu.VMEM((span, per, cols), BF16),
+                pltpu.VMEM((span, per, cols), BF16),
                 pltpu.VMEM((n_fs, rows, width), F32),
                 pltpu.VMEM((n_fs, rows, width), F32),
                 pltpu.VMEM((n_fs, down_rows, cols), F32),
@@ -475,7 +493,7 @@
                 pltpu.VMEM((groups, span, span * quarter, cols), BF16),
                 pltpu.VMEM((groups, span * quarter, cols), BF16),
                 pltpu.VMEM((n_fs * quarter, cols), BF16),
-                dma((6,)),
+                dma((10,)),
                 dma((3, n_fs)),
                 dma((3, n_fs)),
                 dma((3, n_fs)),

time: 152 us -> 151 us (level)
  no operation moved by 1% of the time
where the time goes in v3:
time: 151 us
  Pallas kernels  148 us (98%)
  local copies, waits for them, and re-layouts  2.01 us (1%)
    pallas_call x1, Pallas kernels, on_device(): pl.pallas_call(functools.partial(kernel, n_fs, n_tp, span), out_shape=out...  146 us

profile of v3, /device:TPU:34, one launch (start us, length us, event | category | flops | bytes accessed | tf_op | source)
XLA Modules:
  0.0 150.8 jit_solution(5283631523616085034)
XLA Ops:
  0.6 0.0 copy-start
  0.6 0.7 copy-done
  1.3 0.0 copy-start.1
  1.3 0.7 copy-done.1
  2.0 0.0 copy-start.2
  2.0 0.7 copy-done.2
  2.7 146.4 %experts.1 = (bf16[2,2048,128]{2,1,0:T(8,128)(2,1)S(1)}, bf16[2,2048,128]{2,1,0:T(8,128)(2,1)S(1)}, bf16[2,1024,256]{2,1,0:T(8,128)(2,1)S(1)}, bf16[256,256]{1,0:T(8,128)(2,1)S(1)}) custom-call(bf16[256,2048]{1,0:T(8,128)(2,1)} %tok_hbm.1, s32[2,256]{1,0:T(2,128)S(1)} %bitcast.6, f32[2,256]{1,0:T(2,128)S(1)} %bitcast.7, f32[1,128]{1,0:T(1,128)S(1)} %bitcast.8, ...), custom_call_target="tpu_custom_call" | custom-call | tf_op jit(solution)/shard_map/experts/pallas_call | solution.py:463
  149.0 1.7 %write_out.1 = (bf16[2,2048,128]{2,1,0:T(8,128)(2,1)}, bf16[2,2048,128]{2,1,0:T(8,128)(2,1)}, bf16[2,1024,256]{2,1,0:T(8,128)(2,1)}, bf16[256,256]{1,0:T(8,128)(2,1)}) custom-call(bf16[2,2048,128]{2,1,0:T(8,128)(2,1)S(1)} %get-tuple-element.8.refs_0_, bf16[2,2048,128]{2,1,0:T(8,128)(2,1)S(1)} %get-tuple-element.9.refs_1_, ...), custom_call_target="tpu_custom_call" | custom-call | tf_op jit(solution)/shard_map/write_out/pallas_call | solution.py:527
Async XLA Ops:
  0.6 0.7 copy-start
  1.3 0.7 copy-start.1
  2.0 0.7 copy-start.2

commit v4 on v3

--- a/solution.py
+++ b/solution.py
@@ -23,9 +23,9 @@
 
 def kernel(
     n_fs, n_tp, span,
-    tok_hbm, ids_hbm, rw_hbm, gain_hbm, gm_ref, um_ref, dm_ref,
+    tok_hbm, small_hbm, gm_ref, um_ref, dm_ref,
     og, ou, od, mix_ref,
-    tok_ref, ids_ref, rw_ref, gain_ref, own_part, own_in,
+    tok_ref, small_ref, own_part, own_in,
     g_in, u_in, d_in, g_own, u_own, d_own, g_send, u_send, d_send,
     s_buf, w_send, x_buf, w_recv, h_buf, w_rows, pick, spread, part, gathered, total, final,
     load_sem, z_send, z_recv, y_send, y_recv, w_sems, t_send, t_recv,
@@ -78,7 +78,7 @@
     small = [
         pltpu.make_async_copy(a, b, load_sem.at[6 + i])
         for i, (a, b) in enumerate(
-            ((ids_hbm, ids_ref), (rw_hbm, rw_ref), (gain_hbm, gain_ref), (tok_hbm, tok_ref))
+            ((small_hbm, small_ref), (tok_hbm, tok_ref))
         )
     ]
     for load in small + loads:
@@ -86,25 +86,24 @@
 
     for load in small:
         load.wait()
-    ids = ids_ref[...]
-    first, second = ids[0:1], ids[1:2]
-    group = lax.shift_right_logical(first, GROUP_SIZE.bit_length() - 1)
-    group_hot = (group == lax.broadcasted_iota(jnp.int32, (8, toks), 0)).astype(F32)
+    first, second = small_ref[0:1], small_ref[1:2]
+    group = jnp.floor(first * (1.0 / GROUP_SIZE))
+    group_hot = (group == lax.broadcasted_iota(jnp.int32, (8, toks), 0).astype(F32)).astype(F32)
     row = lax.broadcasted_iota(jnp.int32, (toks, toks), 0)
     col = lax.broadcasted_iota(jnp.int32, (toks, toks), 1)
     counts = jnp.dot(
         group_hot.astype(BF16), (row < col).astype(BF16), preferred_element_type=F32
     )
     rank = jnp.sum(counts * group_hot, axis=0, keepdims=True)
-    target = group.astype(F32) * per + rank
+    target = group * per + rank
     place = (target == row.astype(F32)).astype(BF16)
     tok = tok_ref[...].astype(F32)
     scale = lax.rsqrt(jnp.mean(tok * tok, axis=1, keepdims=True) + 1e-06)
     own = tok_ref[:, pl.ds(pl.multiple_of(t * cols, cols), cols)].astype(F32)
     normed = (own * scale).astype(BF16)
     s_buf[...] = jnp.dot(place, normed, preferred_element_type=F32).astype(BF16)
-    rw = rw_ref[...]
-    expert = lax.broadcasted_iota(jnp.int32, (2 * n_fs, toks), 0)
+    rw = small_ref[2:4]
+    expert = lax.broadcasted_iota(jnp.int32, (2 * n_fs, toks), 0).astype(F32)
     by_expert = jnp.where(first == expert, rw[0:1], 0.0) + jnp.where(second == expert, rw[1:2], 0.0)
     rank_hot = (rank == lax.broadcasted_iota(jnp.int32, (128, toks), 0).astype(F32)).astype(F32)
     w_all = lax.dot_general(
@@ -140,7 +139,7 @@
 
     lax.fori_loop(0, n_fs - 1, dispatch, 0)
 
-    gain_row = gain_ref[...]
+    gain_row = small_ref[4:5, : g_own.shape[0]]
     side = gain_row.shape[1]
     diagonal = lax.broadcasted_iota(jnp.int32, (side, side), 0) == lax.broadcasted_iota(
         jnp.int32, (side, side), 1
@@ -460,16 +459,19 @@
             shape((served, n_fs * down_rows, cols), BF16),
             shape((toks, cols), BF16),
         )
+        small = (
+            jnp.pad(route_ids.T.astype(F32), ((0, 6), (0, 0)))
+            + jnp.pad(route_weights.T, ((2, 4), (0, 0)))
+            + jnp.pad(ffn_gain.reshape(1, rows), ((4, 3), (0, toks - rows)))
+        )
         results = pl.pallas_call(
             functools.partial(kernel, n_fs, n_tp, span),
             out_shape=out_shape,
-            in_specs=[hbm] * 7,
+            in_specs=[hbm] * 5,
             out_specs=(vmem,) * 4,
             scratch_shapes=[
                 pltpu.VMEM((toks, d), BF16),
-                pltpu.VMEM((2, toks), jnp.int32),
-                pltpu.VMEM((2, toks), F32),
-                pltpu.VMEM((1, rows), F32),
+                pltpu.VMEM((8, toks), F32),
                 pltpu.VMEM((span, per, cols), BF16),
                 pltpu.VMEM((span, per, cols), BF16),
                 pltpu.VMEM((n_fs, rows, width), F32),
@@ -493,7 +495,7 @@
                 pltpu.VMEM((groups, span, span * quarter, cols), BF16),
                 pltpu.VMEM((groups, span * quarter, cols), BF16),
                 pltpu.VMEM((n_fs * quarter, cols), BF16),
-                dma((10,)),
+                dma((8,)),
                 dma((3, n_fs)),
                 dma((3, n_fs)),
                 dma((3, n_fs)),
@@ -516,9 +518,7 @@
             name="experts",
         )(
             tokens,
-            route_ids.T,
-            route_weights.T,
-            ffn_gain.reshape(1, rows),
+            small,
             gate_master.reshape(n_fs, served, rows, width),
             up_master.reshape(n_fs, served, rows, width),
             down_master.reshape(n_fs, served, down_rows, cols),

time: 151 us -> 151 us (level)
  local copies, waits for them, and re-layouts: 2.01 us -> 0 us
    unnamed x6 -> x0, local copies, waits for them, and re-layouts: 2.01 us -> none
where the time goes in v4:
time: 151 us
  Pallas kernels  149 us (99%)
    pallas_call x1, Pallas kernels, on_device(): pl.pallas_call(functools.partial(kernel, n_fs, n_tp, span), out_shape=out...  147 us

profile of v4, /device:TPU:34, one launch (start us, length us, event | category | flops | bytes accessed | tf_op | source)
XLA Modules:
  0.0 151.2 jit_solution(13653453358692339628)
XLA Ops:
  0.6 0.7 convert_bitcast_fusion
  1.3 0.7 pad_add_fusion.small_hbm
  2.0 147.5 %experts.1 = (bf16[2,2048,128]{2,1,0:T(8,128)(2,1)S(1)}, bf16[2,2048,128]{2,1,0:T(8,128)(2,1)S(1)}, bf16[2,1024,256]{2,1,0:T(8,128)(2,1)S(1)}, bf16[256,256]{1,0:T(8,128)(2,1)S(1)}) custom-call(bf16[256,2048]{1,0:T(8,128)(2,1)} %tok_hbm.1, f32[8,256]{1,0:T(8,128)S(1)} %pad_add_fusion.small_hbm, f32[16,2,128,128]{3,2,1,0:T(8,128)} %bitcast.7, ...), custom_call_target="tpu_custom_call" | custom-call | tf_op jit(solution)/shard_map/experts/pallas_call | solution.py:467
  149.5 1.7 %write_out.1 = (bf16[2,2048,128]{2,1,0:T(8,128)(2,1)}, bf16[2,2048,128]{2,1,0:T(8,128)(2,1)}, bf16[2,1024,256]{2,1,0:T(8,128)(2,1)}, bf16[256,256]{1,0:T(8,128)(2,1)}) custom-call(bf16[2,2048,128]{2,1,0:T(8,128)(2,1)S(1)} %get-tuple-element.8.refs_0_, bf16[2,2048,128]{2,1,0:T(8,128)(2,1)S(1)} %get-tuple-element.9.refs_1_, ...), custom_call_target="tpu_custom_call" | custom-call | tf_op jit(solution)/shard_map/write_out/pallas_call | solution.py:527
